TPU v7x, 128 devices: a whole 4x4x4 slice. The times are simulated.
128 devices in a mesh: sp: 16 (over z, y), dp: 8 (over x, core).
Axes of the slice: x: 4, y: 4, z: 4, core: 2. Of those that a mesh axis runs over, the one named last changes fastest.
Arguments:
- tokens: bfloat16 [8, 5120, 2048], P('dp', 'sp'), may hold values from -6 to 6
- w_query: bfloat16 [2048, 1024], P('dp', 'sp'), may hold values from -0.125 to 0.125
- w_key: bfloat16 [2048, 1024], P('dp', 'sp'), may hold values from -0.125 to 0.125
- w_value: bfloat16 [2048, 1024], P('dp', 'sp'), may hold values from -0.125 to 0.125
- w_output: bfloat16 [1024, 2048], P('sp', 'dp'), may hold values from -0.1875 to 0.1875
- qk_gain: float32 [2, 64], replicated, may hold values from 0.4 to 7
- decay_sums: float32 [8, 16, 5120], P('dp', 'sp'), may hold values from -1024 to 0, as said below
Outputs:
- layer_out: bfloat16 [8, 5120, 2048], P('dp', 'sp')
Inputs may be any that keep to these rules, and one draw needn't show every extreme that they name: `decay_sums`: each row is non-increasing along positions.
All inputs are finite; a program needn't handle non-finite values.
Results may differ from a plain program's by a relative error of at most 0.0075.
The roundings to bfloat16 on the way count: a program that leaves them out, or rounds other values in their place, can miss the bound.
Values may be sent and summed in bfloat16 or wider, within the bound.
No kernel may reach another device: no remote copies, remote signals or barrier semaphores. Data moves between devices by JAX's collectives and lax.ppermute only.
A program may use at most 128 MiB of HBM per device.

v0:
```python
import jax
import jax.numpy as jnp
from jax import lax
from jax.sharding import Mesh
from jax.sharding import PartitionSpec as P

DP = ("dp_0", "dp_1")
SP = ("sp_0", "sp_1")


def piece_ends(length, count):
    lap = length // count
    if lap >= 8:
        lap -= lap % 8
    return [lap * k for k in range(1, count)]


def all_blocks(value, axes, order):
    pieces = value
    for k in order:
        pieces = lax.all_gather(pieces, axes[k])
    done = order[::-1]
    back = [done.index(k) for k in range(len(axes))]
    pieces = pieces.transpose(*back, *range(len(axes), pieces.ndim))
    return pieces.reshape(-1, *value.shape)


def in_order(pieces, dim):
    lengths = list(pieces.shape[1:])
    lengths[dim] *= pieces.shape[0]
    return jnp.moveaxis(pieces, 0, dim).reshape(lengths)


def spread_gather(value, axes, dim):
    split_at = max(range(max(1, value.ndim - 1)), key=lambda d: value.shape[d])
    count, outs = (len(axes), [])
    for leading, section in enumerate(
        jnp.split(value, piece_ends(value.shape[split_at], count), axis=split_at)
    ):
        if section.size:
            order = [(leading - k) % count for k in range(count)]
            outs.append(all_blocks(section, axes, order))
    return in_order(jnp.concatenate(outs, axis=split_at + 1), dim)


def normalize(values):
    values = values.astype(jnp.float32)
    return values * lax.rsqrt(jnp.mean(values * values, axis=-1, keepdims=True) + 1e-06)


def attend(query_unit, key_unit, value_rows, decay_rows):
    length = query_unit.shape[0]
    groups = query_unit.shape[1]
    width = query_unit.shape[2]
    block = min(512, length)

    def one_block(index):
        start = index * block
        query_block = lax.dynamic_slice_in_dim(query_unit, start, block, 0)
        decay_block = lax.dynamic_slice_in_dim(decay_rows, start, block, 1)
        query_place = start + jnp.arange(block, dtype=jnp.int32)

        def fill(column, buffer):
            key_start = column * block
            key_block = lax.dynamic_slice_in_dim(key_unit, key_start, block, 0)
            decay_keys = lax.dynamic_slice_in_dim(decay_rows, key_start, block, 1)
            scores = jnp.einsum(
                "qhd,khd->hqk", query_block, key_block, preferred_element_type=jnp.float32
            )
            scores = scores + decay_block[:, :, None] - decay_keys[:, None, :]
            key_place = key_start + jnp.arange(block, dtype=jnp.int32)
            scores = jnp.where(
                key_place[None, None, :] <= query_place[None, :, None], scores, -jnp.inf
            )
            return lax.dynamic_update_slice_in_dim(buffer, scores, key_start, 2)

        empty = jnp.full((groups, block, length), -jnp.inf, jnp.float32)
        scores = lax.fori_loop(0, index + 1, fill, empty)
        peak = jnp.max(scores, axis=-1, keepdims=True)
        weights = jnp.exp(scores - peak)
        probs = (weights / jnp.sum(weights, axis=-1, keepdims=True)).astype(jnp.bfloat16)

        def gather_values(column, running):
            key_start = column * block
            prob_block = lax.dynamic_slice_in_dim(probs, key_start, block, 2)
            value_block = lax.dynamic_slice_in_dim(value_rows, key_start, block, 0)
            return running + jnp.einsum(
                "hqk,khd->qhd", prob_block, value_block, preferred_element_type=jnp.float32
            )

        zeros = jnp.zeros((block, groups, width), jnp.float32)
        return lax.fori_loop(0, index + 1, gather_values, zeros)

    blocks = lax.map(one_block, jnp.arange(length // block, dtype=jnp.int32))
    return blocks.reshape(length, groups, width)


def on_device(tokens, w_query, w_key, w_value, w_output, qk_gain, decay_sums):
    own_rows = tokens[0]
    decay_rows = decay_sums[0]
    head_group = decay_rows.shape[0]
    head_dim = qk_gain.shape[1]
    stacked = jnp.stack((w_query, w_key, w_value))
    columns, out_columns = (spread_gather(stacked, DP, 1), spread_gather(w_output, DP, 1))
    whole = lax.all_gather(own_rows, SP, axis=0, tiled=True)
    triple = jnp.einsum("td,kdc->ktc", whole, columns, preferred_element_type=jnp.float32).astype(
        jnp.bfloat16
    )
    length = triple.shape[1]
    grouped = triple.reshape(3, length, head_group, head_dim)
    query_unit = (normalize(grouped[0]) * qk_gain[0] * head_dim ** (-0.5)).astype(jnp.bfloat16)
    key_unit = (normalize(grouped[1]) * qk_gain[1]).astype(jnp.bfloat16)
    attended = attend(query_unit, key_unit, grouped[2], decay_rows)
    head_out = normalize(attended).astype(jnp.bfloat16).reshape(length, head_group * head_dim)
    merged = lax.all_to_all(head_out, SP, split_axis=0, concat_axis=1, tiled=True)
    result = jnp.dot(merged, spread_gather(out_columns, SP, 0), preferred_element_type=jnp.float32)
    return result.astype(jnp.bfloat16)[None]


def solution(mesh):
    torus = Mesh(mesh.devices.reshape(4, 4, 4, 2), ("sp_0", "sp_1", "dp_0", "dp_1"))
    in_specs = (P(DP, SP, None), P(DP, SP), P(DP, SP), P(DP, SP), P(SP, DP), P(), P(DP, SP, None))
    out_specs = P(DP, SP, None)
    return jax.shard_map(
        on_device, mesh=torus, in_specs=in_specs, out_specs=out_specs, check_vma=False
    )
```

profile of v0, /device:TPU:0, one launch (start us, length us, event | category | flops | bytes accessed | tf_op | source)
XLA Modules:
  0.0 617.3 jit_solution(8248347875593230595)
XLA Ops:
  8.0 12.3 %all-gather.5 = bf16[128,256]{1,0:T(8,128)(2,1)S(1)} all-gather(bf16[32,256]{1,0:T(8,128)(2,1)S(1)} %get-tuple-element.211), channel_id=7, replica_groups=mesh['sp_0'=4,'sp_1'=4,'dp_0'=4,'dp_1'=2] {'dp_0'}, dimensions={0}, use_global_device_ids=true | all-gather | bytes 81920 | tf_op jit(solution)/shard_map/all_gather | solution.py:21
  24.1 12.0 %all-gather.8 = bf16[8,32,256]{2,1,0:T(8,128)(2,1)S(1)} all-gather(bf16[2,32,256]{2,1,0:T(8,128)(2,1)S(1)} %bitcast.143), channel_id=10, replica_groups=mesh['sp_0'=4,'sp_1'=4,'dp_0'=4,'dp_1'=2] {'dp_0'}, dimensions={0}, use_global_device_ids=true | all-gather | bytes 163840 | tf_op jit(solution)/shard_map/all_gather | solution.py:21
  36.3 16.9 %all_gather.93 = bf16[4,32,2048]{2,1,0:T(8,128)(2,1)} all-gather(bf16[1,32,2048]{2,1,0:T(8,128)(2,1)S(1)} %all_gather.92), channel_id=1, replica_groups=mesh['sp_0'=4,'sp_1'=4,'dp_0'=4,'dp_1'=2] {'sp_0'}, dimensions={0}, use_global_device_ids=true | all-gather | bytes 655360 | tf_op jit(solution)/shard_map/all_gather | solution.py:21
  53.5 16.2 %all_gather.97 = bf16[4,32,2048]{2,1,0:T(8,128)(2,1)} all-gather(bf16[1,32,2048]{2,1,0:T(8,128)(2,1)S(1)} %all_gather.96), channel_id=1, replica_groups=mesh['sp_0'=4,'sp_1'=4,'dp_0'=4,'dp_1'=2] {'sp_1'}, dimensions={0}, use_global_device_ids=true | all-gather | bytes 655360 | tf_op jit(solution)/shard_map/all_gather | solution.py:21
  69.8 12.1 %all-gather = bf16[12,128,64]{1,2,0:T(8,128)(2,1)S(1)} all-gather(bf16[3,128,64]{1,2,0:T(8,128)(2,1)S(1)} %get-tuple-element.209), channel_id=2, replica_groups=mesh['sp_0'=4,'sp_1'=4,'dp_0'=4,'dp_1'=2] {'dp_0'}, dimensions={0}, use_global_device_ids=true | all-gather | bytes 245760 | tf_op jit(solution)/shard_map/all_gather | solution.py:21
  85.9 12.5 %all-gather.3 = bf16[8,3,128,64]{2,3,1,0:T(8,128)(2,1)S(1)} all-gather(bf16[2,3,128,64]{2,3,1,0:T(8,128)(2,1)S(1)} %bitcast.140), channel_id=5, replica_groups=mesh['sp_0'=4,'sp_1'=4,'dp_0'=4,'dp_1'=2] {'dp_0'}, dimensions={0}, use_global_device_ids=true | all-gather | bytes 491520 | tf_op jit(solution)/shard_map/all_gather | solution.py:21
  98.6 51.4 %all-gather.15.cloned.1.call-done = bf16[1,5120,2048]{2,1,0:T(8,128)(2,1)} async-done(((bf16[1,320,2048]{2,1,0:T(8,128)(2,1)}), bf16[1,5120,2048]{2,1,0:T(8,128)(2,1)}) %all-gather.15.cloned.1.call-update) | async-done | bytes 20971536 | tf_op jit(solution)/shard_map/all_gather | solution.py:105
  150.0 11.5 %fusion.23 = bf16[3,5120,64]{1,2,0:T(8,128)(2,1)S(1)} fusion(bf16[3,2048,64]{1,2,0:T(8,128)(2,1)S(1)} %bitcast.136, bf16[1,5120,2048]{2,1,0:T(8,128)(2,1)} %all-gather.15.cloned.1.call-done), kind=kOutput, calls=%fused_computation.30 | convolution fusion | flops 4027514880 | bytes 23724032 | tf_op jit(solution)/shard_map/td,kdc->ktc/dot_general | solution.py:106
  162.3 418.4 %while.33 = (s32[]{:T(128)}, f32[10,512,1,64]{1,3,2,0:T(8,128)S(1)}, s32[10]{0:T(128)S(1)}, bf16[5120,1,64]{0,2,1:T(8,128)(2,1)S(1)}, f32[1,5120]{1,0:T(1,128)},...) while((s32[]{:T(128)}, ...), condition=%wide.region_9.10_spmd, body=%wide.region_2.9_spmd.sunk | while | flops 83918864 | bytes 91718440 | solution.py:94
  165.1 5.3 broadcast.174
  172.4 4.8 reduce_max.10
  177.2 5.6 fusion.60
  192.1 5.3 broadcast.174
  201.5 4.8 reduce_max.10
  206.3 5.7 fusion.60
  222.6 5.3 broadcast.174
  227.9 6.0 while.34
  238.6 5.6 fusion.60
  256.1 5.3 broadcast.174
  261.4 8.1 %while.34 = (s32[]{:T(128)}, f32[1,512,5120]{1,2,0:T(8,128)}, s32[]{:T(128)}, bf16[5120,1,64]{0,2,1:T(8,128)(2,1)S(1)}, bf16[512,1,64]{0,2,1:T(8,128)(2,1)S(1)},...) while((s32[]{:T(128)}, f32[1,512,5120]{1,2,0:T(8,128)}, ...), condition=%wide.region_4.4_spmd.clone, body=%wide.region_3.3_spmd.clone.sunk | while | flops 34604036 | bytes 1197231 | solution.py:78
  274.2 5.6 fusion.60
  285.0 5.2 while.35
  292.9 5.3 broadcast.174
  298.3 10.1 %while.34 = (s32[]{:T(128)}, f32[1,512,5120]{1,2,0:T(8,128)}, s32[]{:T(128)}, bf16[5120,1,64]{0,2,1:T(8,128)(2,1)S(1)}, bf16[512,1,64]{0,2,1:T(8,128)(2,1)S(1)},...) while((s32[]{:T(128)}, f32[1,512,5120]{1,2,0:T(8,128)}, ...), condition=%wide.region_4.4_spmd.clone, body=%wide.region_3.3_spmd.clone.sunk | while | flops 34604036 | bytes 1197231 | solution.py:78
  313.0 5.6 fusion.60
  323.9 6.4 %while.35 = (s32[]{:T(128)}, f32[512,1,64]{0,2,1:T(8,128)S(1)}, s32[]{:T(128)}, bf16[5120,1,64]{0,2,1:T(8,128)(2,1)S(1)}, bf16[1,512,5120]{1,2,0:T(8,128)(2,1)},...) while((s32[]{:T(128)}, f32[512,1,64]{0,2,1:T(8,128)S(1)}, s32[]{:T(128)}, ...), condition=%wide.region_8.8_spmd, body=%wide.region_7.7_spmd.sunk | while | flops 33587204 | bytes 853131 | solution.py:92
  333.1 5.3 broadcast.174
  338.4 12.1 %while.34 = (s32[]{:T(128)}, f32[1,512,5120]{1,2,0:T(8,128)}, s32[]{:T(128)}, bf16[5120,1,64]{0,2,1:T(8,128)(2,1)S(1)}, bf16[512,1,64]{0,2,1:T(8,128)(2,1)S(1)},...) while((s32[]{:T(128)}, f32[1,512,5120]{1,2,0:T(8,128)}, ...), condition=%wide.region_4.4_spmd.clone, body=%wide.region_3.3_spmd.clone.sunk | while | flops 34604036 | bytes 1197231 | solution.py:78
  355.2 5.6 fusion.60
  366.0 7.7 %while.35 = (s32[]{:T(128)}, f32[512,1,64]{0,2,1:T(8,128)S(1)}, s32[]{:T(128)}, bf16[5120,1,64]{0,2,1:T(8,128)(2,1)S(1)}, bf16[1,512,5120]{1,2,0:T(8,128)(2,1)},...) while((s32[]{:T(128)}, f32[512,1,64]{0,2,1:T(8,128)S(1)}, s32[]{:T(128)}, ...), condition=%wide.region_8.8_spmd, body=%wide.region_7.7_spmd.sunk | while | flops 33587204 | bytes 853131 | solution.py:92
  376.5 5.3 broadcast.174
  381.8 14.1 %while.34 = (s32[]{:T(128)}, f32[1,512,5120]{1,2,0:T(8,128)}, s32[]{:T(128)}, bf16[5120,1,64]{0,2,1:T(8,128)(2,1)S(1)}, bf16[512,1,64]{0,2,1:T(8,128)(2,1)S(1)},...) while((s32[]{:T(128)}, f32[1,512,5120]{1,2,0:T(8,128)}, ...), condition=%wide.region_4.4_spmd.clone, body=%wide.region_3.3_spmd.clone.sunk | while | flops 34604036 | bytes 1197231 | solution.py:78
  400.7 5.6 fusion.60
  411.5 9.0 %while.35 = (s32[]{:T(128)}, f32[512,1,64]{0,2,1:T(8,128)S(1)}, s32[]{:T(128)}, bf16[5120,1,64]{0,2,1:T(8,128)(2,1)S(1)}, bf16[1,512,5120]{1,2,0:T(8,128)(2,1)},...) while((s32[]{:T(128)}, f32[512,1,64]{0,2,1:T(8,128)S(1)}, s32[]{:T(128)}, ...), condition=%wide.region_8.8_spmd, body=%wide.region_7.7_spmd.sunk | while | flops 33587204 | bytes 853131 | solution.py:92
  423.3 5.3 broadcast.174
  428.6 16.2 %while.34 = (s32[]{:T(128)}, f32[1,512,5120]{1,2,0:T(8,128)}, s32[]{:T(128)}, bf16[5120,1,64]{0,2,1:T(8,128)(2,1)S(1)}, bf16[512,1,64]{0,2,1:T(8,128)(2,1)S(1)},...) while((s32[]{:T(128)}, f32[1,512,5120]{1,2,0:T(8,128)}, ...), condition=%wide.region_4.4_spmd.clone, body=%wide.region_3.3_spmd.clone.sunk | while | flops 34604036 | bytes 1197231 | solution.py:78
  449.4 5.6 fusion.60
  460.3 10.3 %while.35 = (s32[]{:T(128)}, f32[512,1,64]{0,2,1:T(8,128)S(1)}, s32[]{:T(128)}, bf16[5120,1,64]{0,2,1:T(8,128)(2,1)S(1)}, bf16[1,512,5120]{1,2,0:T(8,128)(2,1)},...) while((s32[]{:T(128)}, f32[512,1,64]{0,2,1:T(8,128)S(1)}, s32[]{:T(128)}, ...), condition=%wide.region_8.8_spmd, body=%wide.region_7.7_spmd.sunk | while | flops 33587204 | bytes 853131 | solution.py:92
  473.3 5.3 broadcast.174
  478.6 18.2 %while.34 = (s32[]{:T(128)}, f32[1,512,5120]{1,2,0:T(8,128)}, s32[]{:T(128)}, bf16[5120,1,64]{0,2,1:T(8,128)(2,1)S(1)}, bf16[512,1,64]{0,2,1:T(8,128)(2,1)S(1)},...) while((s32[]{:T(128)}, f32[1,512,5120]{1,2,0:T(8,128)}, ...), condition=%wide.region_4.4_spmd.clone, body=%wide.region_3.3_spmd.clone.sunk | while | flops 34604036 | bytes 1197231 | solution.py:78
  501.6 5.6 fusion.60
  512.4 11.6 %while.35 = (s32[]{:T(128)}, f32[512,1,64]{0,2,1:T(8,128)S(1)}, s32[]{:T(128)}, bf16[5120,1,64]{0,2,1:T(8,128)(2,1)S(1)}, bf16[1,512,5120]{1,2,0:T(8,128)(2,1)},...) while((s32[]{:T(128)}, f32[512,1,64]{0,2,1:T(8,128)S(1)}, s32[]{:T(128)}, ...), condition=%wide.region_8.8_spmd, body=%wide.region_7.7_spmd.sunk | while | flops 33587204 | bytes 853131 | solution.py:92
  526.8 5.3 broadcast.174
  532.1 20.2 %while.34 = (s32[]{:T(128)}, f32[1,512,5120]{1,2,0:T(8,128)}, s32[]{:T(128)}, bf16[5120,1,64]{0,2,1:T(8,128)(2,1)S(1)}, bf16[512,1,64]{0,2,1:T(8,128)(2,1)S(1)},...) while((s32[]{:T(128)}, f32[1,512,5120]{1,2,0:T(8,128)}, ...), condition=%wide.region_4.4_spmd.clone, body=%wide.region_3.3_spmd.clone.sunk | while | flops 34604036 | bytes 1197231 | solution.py:78
  557.0 5.6 fusion.60
  567.8 12.9 %while.35 = (s32[]{:T(128)}, f32[512,1,64]{0,2,1:T(8,128)S(1)}, s32[]{:T(128)}, bf16[5120,1,64]{0,2,1:T(8,128)(2,1)S(1)}, bf16[1,512,5120]{1,2,0:T(8,128)(2,1)},...) while((s32[]{:T(128)}, f32[512,1,64]{0,2,1:T(8,128)S(1)}, s32[]{:T(128)}, ...), condition=%wide.region_8.8_spmd, body=%wide.region_7.7_spmd.sunk | while | flops 33587204 | bytes 853131 | solution.py:92
  586.7 5.3 all-to-all-start
  593.8 12.8 %all-to-all-done = bf16[16,320,64]{1,2,0:T(8,128)(2,1)S(1)} async-done(((bf16[16,320,64]{1,2,0:T(8,128)(2,1)}), bf16[16,320,64]{1,2,0:T(8,128)(2,1)S(1)}, u32[]{:S(2)}, u32[]{:S(2)}) %all-to-all-start) | async-done | bytes 655392 | tf_op jit(solution)/shard_map/all_to_all | solution.py:115
  (361 shorter events, 320.1 us)
Async XLA Ops:
  6.5 143.5 %all-gather.15.cloned.1.call-start = ((), (), s32[]{:S(2)}) async-start(), calls=%async_computation.1 | async-start | bytes 22282240 | tf_op jit(solution)/shard_map/all_gather | solution.py:105
  7.3 584.8 %all-gather.17.cloned.1.call-start = ((), (), s32[]{:S(2)}) async-start(), calls=%async_computation.2 | async-start | bytes 2621440 | tf_op jit(solution)/shard_map/all_gather | solution.py:21
  36.1 33.6 %copy-start.1 = (bf16[256,64]{0,1:T(8,128)(2,1)S(1)}, bf16[256,64]{0,1:T(8,128)(2,1)}, u32[]{:S(2)}) copy-start(bf16[256,64]{0,1:T(8,128)(2,1)} %param.16) | copy-start | bytes 98308
  36.1 33.6 %copy-start.2 = (bf16[256,64]{0,1:T(8,128)(2,1)S(1)}, bf16[256,64]{0,1:T(8,128)(2,1)}, u32[]{:S(2)}) copy-start(bf16[256,64]{0,1:T(8,128)(2,1)} %param.15) | copy-start | bytes 98308
  36.1 33.6 %copy-start.3 = (bf16[256,64]{0,1:T(8,128)(2,1)S(1)}, bf16[256,64]{0,1:T(8,128)(2,1)}, u32[]{:S(2)}) copy-start(bf16[256,64]{0,1:T(8,128)(2,1)} %param.14) | copy-start | bytes 98308
  53.3 540.5 %all-gather.19.cloned.1.call-start = ((), (), s32[]{:S(2)}) async-start(), calls=%async_computation.3 | async-start | bytes 2621440 | tf_op jit(solution)/shard_map/all_gather | solution.py:21
  84.0 14.6 %copy-start.4 = (f32[2,64]{1,0:T(2,128)S(1)}, f32[2,64]{1,0:T(2,128)}, u32[]{:S(2)}) copy-start(f32[2,64]{1,0:T(2,128)} %param.18) | copy-start | bytes 1540
  177.2 7.0 %copy-start = (f32[1,512,5120]{1,2,0:T(8,128)S(1)}, f32[1,512,5120]{1,2,0:T(8,128)}, u32[]{:S(2)}) copy-start(f32[1,512,5120]{1,2,0:T(8,128)} %get-tuple-element.359) | copy-start | bytes 31457284 | tf_op jit(solution)/shard_map/while
  206.3 7.1 %copy-start = (f32[1,512,5120]{1,2,0:T(8,128)S(1)}, f32[1,512,5120]{1,2,0:T(8,128)}, u32[]{:S(2)}) copy-start(f32[1,512,5120]{1,2,0:T(8,128)} %get-tuple-element.359) | copy-start | bytes 31457284 | tf_op jit(solution)/shard_map/while
  238.6 7.0 %copy-start = (f32[1,512,5120]{1,2,0:T(8,128)S(1)}, f32[1,512,5120]{1,2,0:T(8,128)}, u32[]{:S(2)}) copy-start(f32[1,512,5120]{1,2,0:T(8,128)} %get-tuple-element.359) | copy-start | bytes 31457284 | tf_op jit(solution)/shard_map/while
  274.2 7.0 %copy-start = (f32[1,512,5120]{1,2,0:T(8,128)S(1)}, f32[1,512,5120]{1,2,0:T(8,128)}, u32[]{:S(2)}) copy-start(f32[1,512,5120]{1,2,0:T(8,128)} %get-tuple-element.359) | copy-start | bytes 31457284 | tf_op jit(solution)/shard_map/while
  313.0 7.0 %copy-start = (f32[1,512,5120]{1,2,0:T(8,128)S(1)}, f32[1,512,5120]{1,2,0:T(8,128)}, u32[]{:S(2)}) copy-start(f32[1,512,5120]{1,2,0:T(8,128)} %get-tuple-element.359) | copy-start | bytes 31457284 | tf_op jit(solution)/shard_map/while
  355.2 7.0 %copy-start = (f32[1,512,5120]{1,2,0:T(8,128)S(1)}, f32[1,512,5120]{1,2,0:T(8,128)}, u32[]{:S(2)}) copy-start(f32[1,512,5120]{1,2,0:T(8,128)} %get-tuple-element.359) | copy-start | bytes 31457284 | tf_op jit(solution)/shard_map/while
  400.7 7.0 %copy-start = (f32[1,512,5120]{1,2,0:T(8,128)S(1)}, f32[1,512,5120]{1,2,0:T(8,128)}, u32[]{:S(2)}) copy-start(f32[1,512,5120]{1,2,0:T(8,128)} %get-tuple-element.359) | copy-start | bytes 31457284 | tf_op jit(solution)/shard_map/while
  449.4 7.0 %copy-start = (f32[1,512,5120]{1,2,0:T(8,128)S(1)}, f32[1,512,5120]{1,2,0:T(8,128)}, u32[]{:S(2)}) copy-start(f32[1,512,5120]{1,2,0:T(8,128)} %get-tuple-element.359) | copy-start | bytes 31457284 | tf_op jit(solution)/shard_map/while
  501.6 7.0 %copy-start = (f32[1,512,5120]{1,2,0:T(8,128)S(1)}, f32[1,512,5120]{1,2,0:T(8,128)}, u32[]{:S(2)}) copy-start(f32[1,512,5120]{1,2,0:T(8,128)} %get-tuple-element.359) | copy-start | bytes 31457284 | tf_op jit(solution)/shard_map/while
  557.0 7.0 %copy-start = (f32[1,512,5120]{1,2,0:T(8,128)S(1)}, f32[1,512,5120]{1,2,0:T(8,128)}, u32[]{:S(2)}) copy-start(f32[1,512,5120]{1,2,0:T(8,128)} %get-tuple-element.359) | copy-start | bytes 31457284 | tf_op jit(solution)/shard_map/while
  586.7 19.9 %all-to-all-start = ((bf16[16,320,64]{1,2,0:T(8,128)(2,1)}), bf16[16,320,64]{1,2,0:T(8,128)(2,1)S(1)}, u32[]{:S(2)}, u32[]{:S(2)}) async-start(bf16[16,320,64]{1,2,0:T(8,128)(2,1)} %fusion.39), calls=%async_computation | async-start | bytes 1572864 | tf_op jit(solution)/shard_map/all_to_all | solution.py:115
Sparse Core Ops, SparseCore 0:
  9.5 140.5 all-gather.14
  151.7 29.9 all-gather.16
  183.3 30.9 all-gather.18
where the time goes:
time: 623 us; the launch traced here: 617 us
  matrix products  158 us (25%)
  other arithmetic  145 us (23%)
  local copies, waits for them, and re-layouts  124 us (20%)
  blocking collectives  89.7 us (14%)
  waiting for transfers between devices  65 us (10%)
  loops' own time  16 us (3%)
  between operations  13.4 us (2%)
    all_gather x10, blocking collectives, all_blocks(): pieces = lax.all_gather(pieces, axes[k])  89.7 us
    dot_general x55, matrix products, fill(): jnp.einsum('qhd,khd->hqk', query_block, key_block, preferred_element_type...  73.3 us
    dot_general x55, matrix products, gather_values(): jnp.einsum('hqk,khd->qhd', prob_block, value_block, preferred_element_typ...  69 us
    reduce_sum x10, other arithmetic, one_block(): jnp.sum(weights, axis=-1, keepdims=True)  55.7 us
    another operation x20, local copies, waits for them, and re-layouts  53.3 us
    all_gather x1, waiting for transfers between devices, on_device(): whole = lax.all_gather(own_rows, SP, axis=0, tiled=True)  51.4 us
    reduce_max x10, other arithmetic, one_block(): peak = jnp.max(scores, axis=-1, keepdims=True)  47.3 us
    convert_element_type x10, other arithmetic, one_block(): (weights / jnp.sum(weights, axis=-1, keepdims=True)).astype(jnp.bfloat16)  38.4 us
  transfers between devices with their start and end apart: 4, of which 2 were waited for; matrix products, arithmetic and copies ran while one was open for 66% of the time, Pallas kernels for 0%

commit v1 on v0

--- a/solution.py
+++ b/solution.py
@@ -102,7 +102,9 @@
     head_dim = qk_gain.shape[1]
     stacked = jnp.stack((w_query, w_key, w_value))
     columns, out_columns = (spread_gather(stacked, DP, 1), spread_gather(w_output, DP, 1))
-    whole = lax.all_gather(own_rows, SP, axis=0, tiled=True)
+    whole = jnp.concatenate(
+        lax.all_to_all(jnp.stack([own_rows] * lax.axis_size(SP)), SP, 0, 0), axis=0
+    )
     triple = jnp.einsum("td,kdc->ktc", whole, columns, preferred_element_type=jnp.float32).astype(
         jnp.bfloat16
     )

time: 623 us -> 868 us (1.39)
  blocking collectives: 89.7 us -> 362 us
  waiting for transfers between devices: 65 us -> 11.4 us
  local copies, waits for them, and re-layouts: 124 us -> 140 us
  starting transfers between devices: 5.39 us -> 15.4 us
    all_gather x10, blocking collectives: 89.7 us -> 362 us  [all_blocks(): pieces = lax.all_gather(pieces, axes[k])]
    all_gather x1 -> x0, waiting for transfers between devices: 51.4 us -> none  [on_device(): whole = lax.all_gather(own_rows, SP, axis=0, tiled=True)]
    another operation x20 -> x21, local copies, waits for them, and re-layouts: 53.3 us -> 61.6 us
  transfers between devices with their start and end apart: 4 -> 4, of which waited for: 2 -> 1; matrix products, arithmetic and copies ran while one was open for 66% -> 48% of each run, Pallas kernels for 0% -> 0%
where the time goes in v1:
time: 868 us; the launch traced here: 862 us
  blocking collectives  362 us (42%)
  matrix products  158 us (18%)
  other arithmetic  146 us (17%)
  local copies, waits for them, and re-layouts  140 us (16%)
  loops' own time  15.8 us (2%)
  starting transfers between devices  15.4 us (2%)
  between operations  13.7 us (2%)
  waiting for transfers between devices  11.4 us (1%)
    all_gather x10, blocking collectives, all_blocks(): pieces = lax.all_gather(pieces, axes[k])  362 us
    dot_general x55, matrix products, fill(): jnp.einsum('qhd,khd->hqk', query_block, key_block, preferred_element_type...  73.2 us
    dot_general x55, matrix products, gather_values(): jnp.einsum('hqk,khd->qhd', prob_block, value_block, preferred_element_typ...  69 us
    reduce_sum x10, other arithmetic, one_block(): jnp.sum(weights, axis=-1, keepdims=True)  55.6 us
    another operation x20, local copies, waits for them, and re-layouts  53.3 us
    reduce_max x10, other arithmetic, one_block(): peak = jnp.max(scores, axis=-1, keepdims=True)  47.1 us
    convert_element_type x10, other arithmetic, one_block(): (weights / jnp.sum(weights, axis=-1, keepdims=True)).astype(jnp.bfloat16)  38.4 us
    dynamic_slice x55, local copies, waits for them, and re-layouts, fill(): decay_keys = lax.dynamic_slice_in_dim(decay_rows, key_start, block, 1)  37.5 us
  transfers between devices with their start and end apart: 4, of which 1 were waited for; matrix products, arithmetic and copies ran while one was open for 48% of the time, Pallas kernels for 0%

profile of v1, /device:TPU:0, one launch (start us, length us, event | category | flops | bytes accessed | tf_op | source)
XLA Modules:
  0.0 862.1 jit_solution(8069791129823999420)
XLA Ops:
  6.5 8.3 stack.19
  14.8 8.3 all-to-all-start
  23.2 12.2 %all-gather.4 = bf16[128,256]{1,0:T(8,128)(2,1)S(1)} all-gather(bf16[32,256]{1,0:T(8,128)(2,1)S(1)} %get-tuple-element.211), channel_id=6, replica_groups=mesh['sp_0'=4,'sp_1'=4,'dp_0'=4,'dp_1'=2] {'dp_0'}, dimensions={0}, use_global_device_ids=true | all-gather | bytes 81920 | tf_op jit(solution)/shard_map/all_gather | solution.py:21
  39.2 12.0 %all-gather.7 = bf16[8,32,256]{2,1,0:T(8,128)(2,1)S(1)} all-gather(bf16[2,32,256]{2,1,0:T(8,128)(2,1)S(1)} %bitcast.141), channel_id=9, replica_groups=mesh['sp_0'=4,'sp_1'=4,'dp_0'=4,'dp_1'=2] {'dp_0'}, dimensions={0}, use_global_device_ids=true | all-gather | bytes 163840 | tf_op jit(solution)/shard_map/all_gather | solution.py:21
  51.4 228.1 %all_gather.89 = bf16[4,32,2048]{2,1,0:T(8,128)(2,1)} all-gather(bf16[1,32,2048]{2,1,0:T(8,128)(2,1)S(1)} %all_gather.88), channel_id=1, replica_groups=mesh['sp_0'=4,'sp_1'=4,'dp_0'=4,'dp_1'=2] {'sp_0'}, dimensions={0}, use_global_device_ids=true | all-gather | bytes 655360 | tf_op jit(solution)/shard_map/all_gather | solution.py:21
  279.7 76.9 %all_gather.93 = bf16[4,32,2048]{2,1,0:T(8,128)(2,1)} all-gather(bf16[1,32,2048]{2,1,0:T(8,128)(2,1)S(1)} %all_gather.92), channel_id=1, replica_groups=mesh['sp_0'=4,'sp_1'=4,'dp_0'=4,'dp_1'=2] {'sp_1'}, dimensions={0}, use_global_device_ids=true | all-gather | bytes 655360 | tf_op jit(solution)/shard_map/all_gather | solution.py:21
  356.7 12.5 %all-gather = bf16[12,128,64]{1,2,0:T(8,128)(2,1)S(1)} all-gather(bf16[3,128,64]{1,2,0:T(8,128)(2,1)S(1)} %get-tuple-element.209), channel_id=2, replica_groups=mesh['sp_0'=4,'sp_1'=4,'dp_0'=4,'dp_1'=2] {'dp_0'}, dimensions={0}, use_global_device_ids=true | all-gather | bytes 245760 | tf_op jit(solution)/shard_map/all_gather | solution.py:21
  373.1 12.5 %all-gather.3 = bf16[8,3,128,64]{2,3,1,0:T(8,128)(2,1)S(1)} all-gather(bf16[2,3,128,64]{2,3,1,0:T(8,128)(2,1)S(1)} %bitcast.138), channel_id=5, replica_groups=mesh['sp_0'=4,'sp_1'=4,'dp_0'=4,'dp_1'=2] {'dp_0'}, dimensions={0}, use_global_device_ids=true | all-gather | bytes 491520 | tf_op jit(solution)/shard_map/all_gather | solution.py:21
  385.9 11.4 %fusion.18 = bf16[3,5120,64]{1,2,0:T(8,128)(2,1)S(1)} fusion(bf16[3,2048,64]{1,2,0:T(8,128)(2,1)S(1)} %bitcast.134, bf16[5120,2048,1]{1,0,2:T(8,128)(2,1)} %bitcast.18), kind=kOutput, calls=%fused_computation.28 | convolution fusion | flops 4027514880 | bytes 23724032 | tf_op jit(solution)/shard_map/td,kdc->ktc/dot_general | solution.py:108
  398.1 424.4 %while.33 = (s32[]{:T(128)}, f32[10,512,1,64]{1,3,2,0:T(8,128)}, s32[10]{0:T(128)S(1)}, bf16[5120,1,64]{0,2,1:T(8,128)(2,1)S(1)}, f32[1,5120]{1,0:T(1,128)}, /*i...) while((s32[]{:T(128)}, f32[10,512,1,64]{1,3,2,0:T(8,128)}, ...), condition=%wide.region_9.10_spmd, body=%wide.region_2.9_spmd.sunk | while | flops 83918864 | bytes 91718952 | solution.py:94
  400.9 5.3 broadcast.175
  408.2 4.7 reduce_max.10
  412.9 5.6 fusion.54
  428.4 5.3 broadcast.175
  442.5 5.6 fusion.54
  459.3 5.3 broadcast.175
  464.6 6.0 while.34
  475.4 5.6 fusion.54
  493.4 5.3 broadcast.175
  498.8 8.1 while.34
  511.5 5.6 fusion.54
  522.4 5.2 while.35
  530.9 5.3 broadcast.175
  536.2 10.1 %while.34 = (s32[]{:T(128)}, f32[1,512,5120]{1,2,0:T(8,128)}, s32[]{:T(128)}, bf16[5120,1,64]{0,2,1:T(8,128)(2,1)S(1)}, bf16[512,1,64]{0,2,1:T(8,128)(2,1)S(1)},...) while((s32[]{:T(128)}, f32[1,512,5120]{1,2,0:T(8,128)}, ...), condition=%wide.region_4.4_spmd.clone, body=%wide.region_3.3_spmd.clone.sunk | while | flops 34604036 | bytes 1197231 | solution.py:78
  551.0 5.6 fusion.54
  561.8 6.4 while.35
  571.7 5.3 broadcast.175
  577.0 12.1 %while.34 = (s32[]{:T(128)}, f32[1,512,5120]{1,2,0:T(8,128)}, s32[]{:T(128)}, bf16[5120,1,64]{0,2,1:T(8,128)(2,1)S(1)}, bf16[512,1,64]{0,2,1:T(8,128)(2,1)S(1)},...) while((s32[]{:T(128)}, f32[1,512,5120]{1,2,0:T(8,128)}, ...), condition=%wide.region_4.4_spmd.clone, body=%wide.region_3.3_spmd.clone.sunk | while | flops 34604036 | bytes 1197231 | solution.py:78
  593.8 5.6 fusion.54
  604.6 7.7 while.35
  615.7 5.3 broadcast.175
  621.1 14.1 %while.34 = (s32[]{:T(128)}, f32[1,512,5120]{1,2,0:T(8,128)}, s32[]{:T(128)}, bf16[5120,1,64]{0,2,1:T(8,128)(2,1)S(1)}, bf16[512,1,64]{0,2,1:T(8,128)(2,1)S(1)},...) while((s32[]{:T(128)}, f32[1,512,5120]{1,2,0:T(8,128)}, ...), condition=%wide.region_4.4_spmd.clone, body=%wide.region_3.3_spmd.clone.sunk | while | flops 34604036 | bytes 1197231 | solution.py:78
  639.9 5.6 fusion.54
  650.7 9.0 %while.35 = (s32[]{:T(128)}, f32[512,1,64]{0,2,1:T(8,128)S(1)}, s32[]{:T(128)}, bf16[5120,1,64]{0,2,1:T(8,128)(2,1)S(1)}, bf16[1,512,5120]{1,2,0:T(8,128)(2,1)},...) while((s32[]{:T(128)}, f32[512,1,64]{0,2,1:T(8,128)S(1)}, s32[]{:T(128)}, ...), condition=%wide.region_8.8_spmd, body=%wide.region_7.7_spmd.sunk | while | flops 33587204 | bytes 853131 | solution.py:92
  663.1 5.3 broadcast.175
  668.4 16.1 %while.34 = (s32[]{:T(128)}, f32[1,512,5120]{1,2,0:T(8,128)}, s32[]{:T(128)}, bf16[5120,1,64]{0,2,1:T(8,128)(2,1)S(1)}, bf16[512,1,64]{0,2,1:T(8,128)(2,1)S(1)},...) while((s32[]{:T(128)}, f32[1,512,5120]{1,2,0:T(8,128)}, ...), condition=%wide.region_4.4_spmd.clone, body=%wide.region_3.3_spmd.clone.sunk | while | flops 34604036 | bytes 1197231 | solution.py:78
  689.3 5.6 fusion.54
  700.1 10.3 %while.35 = (s32[]{:T(128)}, f32[512,1,64]{0,2,1:T(8,128)S(1)}, s32[]{:T(128)}, bf16[5120,1,64]{0,2,1:T(8,128)(2,1)S(1)}, bf16[1,512,5120]{1,2,0:T(8,128)(2,1)},...) while((s32[]{:T(128)}, f32[512,1,64]{0,2,1:T(8,128)S(1)}, s32[]{:T(128)}, ...), condition=%wide.region_8.8_spmd, body=%wide.region_7.7_spmd.sunk | while | flops 33587204 | bytes 853131 | solution.py:92
  713.8 5.3 broadcast.175
  719.1 18.2 %while.34 = (s32[]{:T(128)}, f32[1,512,5120]{1,2,0:T(8,128)}, s32[]{:T(128)}, bf16[5120,1,64]{0,2,1:T(8,128)(2,1)S(1)}, bf16[512,1,64]{0,2,1:T(8,128)(2,1)S(1)},...) while((s32[]{:T(128)}, f32[1,512,5120]{1,2,0:T(8,128)}, ...), condition=%wide.region_4.4_spmd.clone, body=%wide.region_3.3_spmd.clone.sunk | while | flops 34604036 | bytes 1197231 | solution.py:78
  742.1 5.6 fusion.54
  752.9 11.6 %while.35 = (s32[]{:T(128)}, f32[512,1,64]{0,2,1:T(8,128)S(1)}, s32[]{:T(128)}, bf16[5120,1,64]{0,2,1:T(8,128)(2,1)S(1)}, bf16[1,512,5120]{1,2,0:T(8,128)(2,1)},...) while((s32[]{:T(128)}, f32[512,1,64]{0,2,1:T(8,128)S(1)}, s32[]{:T(128)}, ...), condition=%wide.region_8.8_spmd, body=%wide.region_7.7_spmd.sunk | while | flops 33587204 | bytes 853131 | solution.py:92
  767.9 5.3 broadcast.175
  773.2 20.2 %while.34 = (s32[]{:T(128)}, f32[1,512,5120]{1,2,0:T(8,128)}, s32[]{:T(128)}, bf16[5120,1,64]{0,2,1:T(8,128)(2,1)S(1)}, bf16[512,1,64]{0,2,1:T(8,128)(2,1)S(1)},...) while((s32[]{:T(128)}, f32[1,512,5120]{1,2,0:T(8,128)}, ...), condition=%wide.region_4.4_spmd.clone, body=%wide.region_3.3_spmd.clone.sunk | while | flops 34604036 | bytes 1197231 | solution.py:78
  798.1 5.6 fusion.54
  808.9 12.9 %while.35 = (s32[]{:T(128)}, f32[512,1,64]{0,2,1:T(8,128)S(1)}, s32[]{:T(128)}, bf16[5120,1,64]{0,2,1:T(8,128)(2,1)S(1)}, bf16[1,512,5120]{1,2,0:T(8,128)(2,1)},...) while((s32[]{:T(128)}, f32[512,1,64]{0,2,1:T(8,128)S(1)}, s32[]{:T(128)}, ...), condition=%wide.region_8.8_spmd, body=%wide.region_7.7_spmd.sunk | while | flops 33587204 | bytes 853131 | solution.py:92
  831.1 7.0 all-to-all-start.1
  839.8 11.3 %all-to-all-done.1 = bf16[16,320,64]{1,2,0:T(8,128)(2,1)S(1)} async-done(((bf16[16,320,64]{1,2,0:T(8,128)(2,1)}), bf16[16,320,64]{1,2,0:T(8,128)(2,1)S(1)}, u32[]{:S(2)}, u32[]{:S(2)}) %all-to-all-start.1) | async-done | bytes 655392 | tf_op jit(solution)/shard_map/all_to_all | solution.py:117
  (363 shorter events, 332.4 us)
Async XLA Ops:
  14.8 8.4 copy-start.1
  14.8 371.1 %all-to-all-start = ((bf16[16,320,2048]{2,1,0:T(8,128)(2,1)}), bf16[16,320,2048]{2,1,0:T(8,128)(2,1)}, u32[]{:S(2)}, u32[]{:S(2)}) async-start(bf16[16,320,2048]{2,1,0:T(8,128)(2,1)} %stack.19), calls=%async_computation | async-start | bytes 41943040 | tf_op jit(solution)/shard_map/all_to_all | solution.py:106
  23.1 814.9 %all-gather.13.cloned.1.call-start = ((), (), s32[]{:S(2)}) async-start(), calls=%async_computation.2 | async-start | bytes 2621440 | tf_op jit(solution)/shard_map/all_gather | solution.py:21
  51.2 305.4 %copy-start.2 = (bf16[256,64]{0,1:T(8,128)(2,1)S(1)}, bf16[256,64]{0,1:T(8,128)(2,1)}, u32[]{:S(2)}) copy-start(bf16[256,64]{0,1:T(8,128)(2,1)} %param.16) | copy-start | bytes 98308
  51.2 305.4 %copy-start.3 = (bf16[256,64]{0,1:T(8,128)(2,1)S(1)}, bf16[256,64]{0,1:T(8,128)(2,1)}, u32[]{:S(2)}) copy-start(bf16[256,64]{0,1:T(8,128)(2,1)} %param.15) | copy-start | bytes 98308
  51.2 305.4 %copy-start.4 = (bf16[256,64]{0,1:T(8,128)(2,1)S(1)}, bf16[256,64]{0,1:T(8,128)(2,1)}, u32[]{:S(2)}) copy-start(bf16[256,64]{0,1:T(8,128)(2,1)} %param.14) | copy-start | bytes 98308
  279.5 560.3 %all-gather.15.cloned.1.call-start = ((), (), s32[]{:S(2)}) async-start(), calls=%async_computation.3 | async-start | bytes 2621440 | tf_op jit(solution)/shard_map/all_gather | solution.py:21
  371.2 14.6 %copy-start.5 = (f32[2,64]{1,0:T(2,128)S(1)}, f32[2,64]{1,0:T(2,128)}, u32[]{:S(2)}) copy-start(f32[2,64]{1,0:T(2,128)} %param.18) | copy-start | bytes 1540
  412.9 7.0 copy-start
  442.5 7.0 copy-start
  475.4 7.0 copy-start
  511.5 7.0 copy-start
  551.0 7.0 copy-start
  593.8 7.0 copy-start
  639.9 7.0 copy-start
  689.3 7.0 copy-start
  742.1 7.0 copy-start
  798.1 7.0 copy-start
  831.1 20.0 %all-to-all-start.1 = ((bf16[16,320,64]{1,2,0:T(8,128)(2,1)}), bf16[16,320,64]{1,2,0:T(8,128)(2,1)S(1)}, u32[]{:S(2)}, u32[]{:S(2)}) async-start(bf16[16,320,64]{1,2,0:T(8,128)(2,1)} %fusion.32), calls=%async_computation.1 | async-start | bytes 1572864 | tf_op jit(solution)/shard_map/all_to_all | solution.py:117
Sparse Core Ops, SparseCore 0:
  279.6 72.8 all-gather.12
  356.7 32.2 all-gather.14
